TPU v7x, 32 devices: a whole 2x2x4 slice. The times are simulated.
32 devices in a mesh: sp: 8 (over z, y), tp: 4 (over x, core).
Axes of the slice: x: 2, y: 2, z: 4, core: 2. Of those that a mesh axis runs over, the one named last changes fastest.
Arguments:
- hidden_states: bfloat16 [4096, 4096], P('sp', 'tp'), may hold values from -6 to 6
- pre_gain: float32 [2, 4096], replicated, may hold values from 0.1 to 1.9
- post_gain: float32 [2, 4096], P(None, 'tp'), may hold values from 0.1 to 1.9
- w_value: bfloat16 [2, 4096, 2048], P(None, 'sp', 'tp'), may hold values from -0.09375 to 0.09375
- w_outer: bfloat16 [2, 4096, 2048], P(None, 'sp', 'tp'), may hold values from -0.09375 to 0.09375
- w_inner: bfloat16 [2, 4096, 2048], P(None, 'sp', 'tp'), may hold values from -0.09375 to 0.09375
- taps: float32 [2, 3, 2048], P(None, None, 'tp'), may hold values from -3 to 3
- w_out: bfloat16 [2, 2048, 4096], P(None, 'tp', 'sp'), as said below
Outputs:
- final_states: bfloat16 [4096, 4096], P('sp', 'tp')
Inputs may be any that keep to these rules, and one draw needn't show every extreme that they name: `w_out`: independent entries; the columns fall into 8 groups of 512 consecutive columns, each group with its own scale.
All inputs are finite; a program needn't handle non-finite values.
Results may differ from a plain program's by a relative error of at most 0.024.
Values may be sent and summed in bfloat16 or wider, within the bound.
A program may use at most 128 MiB of HBM per device.

v0:
```python
import jax
import jax.numpy as jnp
from jax import lax
from jax.sharding import PartitionSpec as P

D = 4096


eps = 1e-06


def passed_along(value, axis, by):
    size = lax.axis_size(axis)
    pairs = [(i, i + by) for i in range(size) if 0 <= i + by < size]
    return lax.ppermute(value, axis, pairs)


def local(hidden_states, pre_gain, post_gain, w_value, w_outer, w_inner, taps, w_out):
    current = hidden_states
    layers = w_value.shape[0]
    whole_value, whole_outer, whole_inner, whole_out = (
        lax.all_gather(w_value, "sp", axis=1, tiled=True),
        lax.all_gather(w_outer, "sp", axis=1, tiled=True),
        lax.all_gather(w_inner, "sp", axis=1, tiled=True),
        lax.all_gather(w_out, "sp", axis=2, tiled=True),
    )
    for layer_index in range(layers):
        gathered = lax.all_gather(current, "tp", axis=1, tiled=True)
        widened = gathered.astype(jnp.float32)
        normed = (
            widened
            * lax.rsqrt(jnp.mean(widened * widened, axis=1, keepdims=True) + eps)
            * pre_gain[layer_index]
        ).astype(jnp.bfloat16)
        value_proj = jnp.dot(normed, whole_value[layer_index], preferred_element_type=jnp.float32)
        outer_proj = jnp.dot(normed, whole_outer[layer_index], preferred_element_type=jnp.float32)
        inner_proj = jnp.dot(normed, whole_inner[layer_index], preferred_element_type=jnp.float32)
        gated_input = (inner_proj * value_proj).astype(jnp.bfloat16)
        before = passed_along(gated_input[-2:], "sp", 1)
        extended = jnp.concatenate([before, gated_input], axis=0).astype(jnp.float32)
        length = gated_input.shape[0]
        kernel = taps[layer_index]
        convolved = (
            extended[0:length] * kernel[0]
            + extended[1 : length + 1] * kernel[1]
            + extended[2 : length + 2] * kernel[2]
        )
        conv_out = (outer_proj * convolved).astype(jnp.bfloat16)
        partial_terms = jnp.dot(
            conv_out, whole_out[layer_index], preferred_element_type=jnp.float32
        )
        mixed = lax.psum_scatter(
            partial_terms.astype(jnp.bfloat16), "tp", scatter_dimension=1, tiled=True
        ).astype(jnp.float32)
        power = lax.psum(jnp.sum(mixed * mixed, axis=1), "tp")
        rescale = lax.rsqrt(power / D + eps)
        current = (
            current.astype(jnp.float32) + mixed * rescale[:, None] * post_gain[layer_index]
        ).astype(jnp.bfloat16)
    return current


def solution(mesh):
    placed = (
        P("sp", "tp"),
        P(),
        P(None, "tp"),
        P(None, "sp", "tp"),
        P(None, "sp", "tp"),
        P(None, "sp", "tp"),
        P(None, None, "tp"),
        P(None, "tp", "sp"),
    )
    return jax.shard_map(
        local, mesh=mesh, in_specs=placed, out_specs=P("sp", "tp"), check_vma=False
    )
```

profile of v0, /device:TPU:0, one launch (start us, length us, event | category | flops | bytes accessed | tf_op | source)
XLA Modules:
  0.0 729.6 jit_solution(7224380522898905791)
XLA Ops:
  6.5 0.0 copy-start.3
  6.5 0.0 all-gather.7.cloned.1.call-start
  6.5 0.7 all-gather.7.cloned.1.call-update
  7.3 0.0 all-gather.13.cloned.1.call-start
  7.3 0.7 all-gather.13.cloned.1.call-update
  8.0 0.0 all-gather.11.cloned.1.call-start
  8.1 0.7 all-gather.11.cloned.1.call-update
  8.7 0.0 all-gather.9.cloned.1.call-start
  8.8 0.5 all-gather.9.cloned.1.call-update
  9.3 0.0 all-gather.15.cloned.1.call-start
  9.4 0.5 all-gather.15.cloned.1.call-update
  9.9 0.0 reduce-scatter.3.cloned.1.call-start
  10.0 0.0 copy-done.3
  10.0 36.1 %all-gather.7.cloned.1.call-done = bf16[512,4096]{1,0:T(8,128)(2,1)} async-done(((bf16[512,1024]{1,0:T(8,128)(2,1)}), bf16[512,4096]{1,0:T(8,128)(2,1)}) %all-gather.7.cloned.1.call-update) | async-done | bytes 4194320 | tf_op jit(solution)/shard_map/all_gather | solution.py:28
  46.1 3.1 fusion
  49.2 123.6 %all-gather.13.cloned.1.call-done = bf16[2,4096,512]{2,1,0:T(8,128)(2,1)} async-done(((bf16[2,512,512]{2,1,0:T(8,128)(2,1)}), bf16[2,4096,512]{2,1,0:T(8,128)(2,1)}) %all-gather.13.cloned.1.call-update) | async-done | bytes 8388624 | tf_op jit(solution)/shard_map/all_gather | solution.py:22
  172.8 5.8 fusion.9
  178.6 0.0 copy-start.4
  178.6 119.0 %all-gather.11.cloned.1.call-done = bf16[2,4096,512]{2,1,0:T(8,128)(2,1)} async-done(((bf16[2,512,512]{2,1,0:T(8,128)(2,1)}), bf16[2,4096,512]{2,1,0:T(8,128)(2,1)}) %all-gather.11.cloned.1.call-update) | async-done | bytes 8388624 | tf_op jit(solution)/shard_map/all_gather | solution.py:24
  297.6 5.8 fusion.26
  303.5 2.5 collective-permute-start
  306.0 0.0 copy-done.4
  306.0 1.3 collective-permute-done
  307.3 0.2 maximum_convert_fusion
  307.4 114.9 %all-gather.9.cloned.1.call-done = bf16[2,4096,512]{2,1,0:T(8,128)(2,1)} async-done(((bf16[2,512,512]{2,1,0:T(8,128)(2,1)}), bf16[2,4096,512]{2,1,0:T(8,128)(2,1)}) %all-gather.9.cloned.1.call-update) | async-done | bytes 8388624 | tf_op jit(solution)/shard_map/all_gather | solution.py:23
  422.4 6.0 fusion.27
  428.4 119.0 %all-gather.15.cloned.1.call-done = bf16[2,512,4096]{2,1,0:T(8,128)(2,1)} async-done(((bf16[2,512,512]{2,1,0:T(8,128)(2,1)}), bf16[2,512,4096]{2,1,0:T(8,128)(2,1)}) %all-gather.15.cloned.1.call-update) | async-done | bytes 8388624 | tf_op jit(solution)/shard_map/all_gather | solution.py:25
  547.4 6.7 convolution_convert_fusion.1
  554.1 0.0 copy-start.5
  554.1 0.0 copy-start.2
  554.1 0.0 reduce-scatter.3.cloned.1.call-update
  554.1 0.0 all-gather.17.cloned.1.call-start
  554.1 0.6 copy-done.5
  554.8 42.1 %reduce-scatter.3.cloned.1.call-done = bf16[512,1024]{1,0:T(8,128)(2,1)} async-done(((bf16[512,4096]{1,0:T(8,128)(2,1)}), bf16[512,1024]{1,0:T(8,128)(2,1)}) %reduce-scatter.3.cloned.1.call-update) | async-done | bytes 1048592 | tf_op jit(solution)/shard_map/reduce_scatter | solution.py:52
  596.8 1.5 fusion.12
  598.3 5.8 psum.14
  604.1 0.0 copy-done.2
  604.1 2.6 fusion.15
  606.7 0.0 all-gather.17.cloned.1.call-update
  606.8 0.2 reduce-scatter.5.cloned.1.call-start
  607.0 35.0 %all-gather.17.cloned.1.call-done = bf16[512,4096]{1,0:T(8,128)(2,1)} async-done(((bf16[512,1024]{1,0:T(8,128)(2,1)}), bf16[512,4096]{1,0:T(8,128)(2,1)}) %all-gather.17.cloned.1.call-update) | async-done | bytes 4194320 | tf_op jit(solution)/shard_map/all_gather | solution.py:28
  642.0 0.0 copy-start.1
  642.0 3.2 fusion.3
  645.2 0.2 copy-done.1
  645.4 0.0 slice-start.2
  645.4 4.7 fusion.6
  650.2 0.0 slice-start.3
  650.2 4.7 fusion.24
  655.0 3.4 collective-permute-start.1
  658.3 1.3 collective-permute-done.1
  659.6 0.2 maximum_convert_fusion.1
  659.8 0.0 slice-done.2
  659.8 0.0 slice-done.3
  659.8 0.0 slice-start.1
  659.8 2.6 fusion.25
  662.4 0.0 slice-done
  662.4 0.7 slice-done.1
  663.2 4.3 convolution_convert_fusion
  667.5 0.0 reduce-scatter.5.cloned.1.call-update
  667.5 45.4 %reduce-scatter.5.cloned.1.call-done = bf16[512,1024]{1,0:T(8,128)(2,1)} async-done(((bf16[512,4096]{1,0:T(8,128)(2,1)}), bf16[512,1024]{1,0:T(8,128)(2,1)}) %reduce-scatter.5.cloned.1.call-update) | async-done | bytes 1048592 | tf_op jit(solution)/shard_map/reduce_scatter | solution.py:52
  712.9 1.5 fusion.16
  714.4 5.8 psum.15
  720.1 0.0 copy-done
  720.1 2.6 fusion.19
  (13 shorter events, 0.1 us)
Async XLA Ops:
  6.5 3.4 copy-start.3
  6.5 39.6 %all-gather.7.cloned.1.call-start = ((), (), s32[]{:S(2)}) async-start(), calls=%async_computation.2 | async-start | bytes 5242880 | tf_op jit(solution)/shard_map/all_gather | solution.py:28
  7.3 165.5 %all-gather.13.cloned.1.call-start = ((), (), s32[]{:S(2)}) async-start(), calls=%async_computation.5 | async-start | bytes 9437184 | tf_op jit(solution)/shard_map/all_gather | solution.py:22
  8.0 289.6 %all-gather.11.cloned.1.call-start = ((), (), s32[]{:S(2)}) async-start(), calls=%async_computation.4 | async-start | bytes 9437184 | tf_op jit(solution)/shard_map/all_gather | solution.py:24
  8.7 413.6 %all-gather.9.cloned.1.call-start = ((), (), s32[]{:S(2)}) async-start(), calls=%async_computation.3 | async-start | bytes 9437184 | tf_op jit(solution)/shard_map/all_gather | solution.py:23
  9.3 538.1 %all-gather.15.cloned.1.call-start = ((), (), s32[]{:S(2)}) async-start(), calls=%async_computation.6 | async-start | bytes 9437184 | tf_op jit(solution)/shard_map/all_gather | solution.py:25
  9.9 586.9 %reduce-scatter.3.cloned.1.call-start = ((), (), s32[]{:S(2)}) async-start(), calls=%async_computation.7 | async-start | bytes 5242880 | tf_op jit(solution)/shard_map/reduce_scatter | solution.py:52
  178.6 127.4 %copy-start.4 = (f32[2,3,512]{2,0,1:T(2,128)S(1)}, f32[2,3,512]{2,0,1:T(2,128)}, u32[]{:S(2)}) copy-start(f32[2,3,512]{2,0,1:T(2,128)} %param.14) | copy-start | bytes 36868
  303.5 3.8 collective-permute-start
  554.1 0.7 copy-start.5
  554.1 50.0 %copy-start.2 = (bf16[512,1024]{1,0:T(8,128)(2,1)S(1)}, bf16[512,1024]{1,0:T(8,128)(2,1)}, u32[]{:S(2)}) copy-start(bf16[512,1024]{1,0:T(8,128)(2,1)} %param.8) | copy-start | bytes 3145732
  554.1 87.9 %all-gather.17.cloned.1.call-start = ((), (), s32[]{:S(2)}) async-start(), calls=%async_computation.8 | async-start | bytes 5242880 | tf_op jit(solution)/shard_map/all_gather | solution.py:28
  606.8 106.1 %reduce-scatter.5.cloned.1.call-start = ((), (), s32[]{:S(2)}) async-start(), calls=%async_computation.9 | async-start | bytes 5242880 | tf_op jit(solution)/shard_map/reduce_scatter | solution.py:52
  642.0 3.4 copy-start.1
  645.4 14.4 %slice-start.2 = ((s8[8388608]{0:T(1024)(128)(4,1)}), s8[4194304]{0:T(1024)(128)(4,1)S(1)}, s32[]{:S(2)}) async-start(s8[8388608]{0:T(1024)(128)(4,1)} %bitcast.68), calls=%async_computation.12 | async-start | bytes 8388608
  650.2 9.6 %slice-start.3 = ((s8[8388608]{0:T(1024)(128)(4,1)}), s8[4194304]{0:T(1024)(128)(4,1)S(1)}, s32[]{:S(2)}) async-start(s8[8388608]{0:T(1024)(128)(4,1)} %bitcast.68), calls=%async_computation.13 | async-start | bytes 8388608
  655.0 4.7 collective-permute-start.1
  659.6 2.8 slice-start
  659.8 3.3 slice-start.1
  667.5 52.7 %copy-start = (bf16[512,1024]{1,0:T(8,128)(2,1)S(1)}, bf16[512,1024]{1,0:T(8,128)(2,1)}, u32[]{:S(2)}) copy-start(bf16[512,1024]{1,0:T(8,128)(2,1)} %fusion.15) | copy-start | bytes 3145732
Sparse Core Ops, SparseCore 0:
  8.9 37.1 all-gather.6
  48.3 124.4 all-gather.12
  175.0 122.6 all-gather.10
  299.7 122.6 all-gather.8
  424.2 123.1 all-gather.14
  554.2 42.5 reduce-scatter.2
  606.9 35.0 all-gather.16
  667.6 45.2 reduce-scatter.4
where the time goes:
time: 730 us
  waiting for transfers between devices  641 us (88%)
  matrix products  40.7 us (6%)
  other arithmetic  14.9 us (2%)
  between operations  13.7 us (2%)
  blocking collectives  11.5 us (2%)
    all_gather x1, waiting for transfers between devices, local(): lax.all_gather(w_value, 'sp', axis=1, tiled=True)  124 us
    all_gather x1, waiting for transfers between devices, local(): lax.all_gather(w_out, 'sp', axis=2, tiled=True)  119 us
    all_gather x1, waiting for transfers between devices, local(): lax.all_gather(w_inner, 'sp', axis=1, tiled=True)  119 us
    all_gather x1, waiting for transfers between devices, local(): lax.all_gather(w_outer, 'sp', axis=1, tiled=True)  115 us
    reduce_scatter x2, waiting for transfers between devices, local(): lax.psum_scatter(partial_terms.astype(jnp.bfloat16), 'tp', scatter_dimens...  87.4 us
    all_gather x2, waiting for transfers between devices, local(): gathered = lax.all_gather(current, 'tp', axis=1, tiled=True)  71.1 us
  transfers between devices with their start and end apart: 10, of which 10 were waited for; matrix products, arithmetic and copies ran while one was open for 3% of the time, Pallas kernels for 0%

commit v1 on v0

v1 whole, which is shorter than its diff:
```python
import functools

import jax
import jax.numpy as jnp
from jax import lax
from jax.experimental import pallas as pl
from jax.experimental.pallas import tpu as pltpu
from jax.sharding import PartitionSpec as P

MESH = pl.DeviceIdType.MESH
HALO = 16
eps = 1e-06
F32 = jnp.float32
BF16 = jnp.bfloat16


def kernel(
    SP, TP, h_ref, pre, post, wv, wo, wi, taps, wout, out_ref,
    wbuf, obuf, xbuf, nbuf, pbuf, pa, pb, mixed, gbuf, oubuf, hbuf, cbuf, pw,
    own_sem, sR, rR, sL, rL, sY, rY, sX, rX, sXr, rXr, sA, rA, sB, rB, sP, rP, sH, rH, xsem,
):
    Y = TP // 2
    Z = SP // Y
    X = TP // 2
    s = lax.axis_index("sp")
    t = lax.axis_index("tp")
    z, y = s // Y, s % Y
    x, c = t // 2, t % 2
    L, Ds, Ct = wv.shape
    Tk, Dt = h_ref.shape
    D = Dt * TP
    items = 4 * L
    wrefs = (wi, wv, wo, wout)

    def rcopy(src, dst, ss, rs, dev):
        return pltpu.make_async_remote_copy(
            src_ref=src, dst_ref=dst, send_sem=ss, recv_sem=rs, device_id=dev, device_id_type=MESH
        )

    barrier = pltpu.get_barrier_semaphore()

    def hello(dev):
        pl.semaphore_signal(barrier, inc=1, device_id=dev, device_id_type=MESH)

    for by in (Y, SP - Y, 1, SP - 1):
        hello(((s + by) % SP, t))
    for d in range(1, Y):
        hello((z * Y + (y + d) % Y, t))
    for d in range(1, TP):
        hello((s, (t + d) % TP))
    pl.semaphore_wait(barrier, 4 + Y - 1 + TP - 1)

    def slot(i, b):
        l, m = divmod(i, 4)
        if m < 3:
            return wbuf.at[l, m, pl.ds(pl.multiple_of(b * Ds, Ds), Ds)]
        return obuf.at[l, pl.ds(pl.multiple_of(b * Ct, Ct), Ct)]

    def own(i):
        l, m = divmod(i, 4)
        return wrefs[m].at[l]

    def to_right(i, h, src=None):
        b = slot(i, (z - h) * Y + y)
        return rcopy(b if src is None else src, b, sR.at[i, h], rR.at[i, h], (s + Y, t))

    def to_left(i, h, src=None):
        b = slot(i, (z + h) * Y + y)
        return rcopy(b if src is None else src, b, sL.at[i, h], rL.at[i, h], (s - Y, t))

    def from_left(i, h):
        b = slot(i, (z - 1 - h) * Y + y)
        return rcopy(b, b, sR.at[i, h], rR.at[i, h], (s - Y, t))

    def from_right(i, h):
        b = slot(i, (z + 1 + h) * Y + y)
        return rcopy(b, b, sL.at[i, h], rL.at[i, h], (s + Y, t))

    def across(i, zb, d, src=None):
        b = slot(i, zb * Y + y)
        return rcopy(
            b if src is None else src, b, sY.at[i, zb, d - 1], rY.at[i, zb, d - 1],
            (z * Y + (y + d) % Y, t),
        )

    def from_across(i, zb, d):
        b = slot(i, zb * Y + (y - d + Y) % Y)
        return rcopy(b, b, sY.at[i, zb, d - 1], rY.at[i, zb, d - 1], (z * Y + (y + d) % Y, t))

    def own_copy(i):
        return pltpu.make_async_copy(own(i), slot(i, s), own_sem.at[i])

    def stage(i, h):
        if h == 0:
            @pl.when(z < Z - 1)
            def _():
                to_right(i, 0, own(i)).start()

            @pl.when(z > 0)
            def _():
                to_left(i, 0, own(i)).start()

            for d in range(1, Y):
                across(i, z, d, own(i)).start()
            own_copy(i).start()
            return

        @pl.when(z - h >= 0)
        def _():
            from_left(i, h - 1).wait_recv()
            if h <= Z - 2:
                @pl.when(z < Z - 1)
                def _():
                    to_right(i, h).start()
            for d in range(1, Y):
                across(i, z - h, d).start()

        @pl.when(z + h <= Z - 1)
        def _():
            from_right(i, h - 1).wait_recv()
            if h <= Z - 2:
                @pl.when(z > 0)
                def _():
                    to_left(i, h).start()
            for d in range(1, Y):
                across(i, z + h, d).start()

    def advance(tau):
        for i in range(items):
            if 0 <= tau - i <= Z - 1:
                stage(i, tau - i)

    def arrived(i):
        own_copy(i).wait()
        for zb in range(Z):
            for d in range(1, Y):
                from_across(i, zb, d).wait_recv()

    mate = (s, x * 2 + 1 - c)

    def x_mate(l, src):
        return rcopy(src, xbuf.at[t], sX.at[l, 0], rX.at[l, 0], mate)

    def x_far(l, dx, src):
        return rcopy(src, xbuf.at[t], sX.at[l, dx], rX.at[l, dx], (s, ((x + dx) % X) * 2 + c))

    def x_relay(l, dx):
        b = xbuf.at[((x - dx + X) % X) * 2 + c]
        return rcopy(b, b, sXr.at[l, dx], rXr.at[l, dx], mate)

    def gather_start(l, src):
        for dx in range(1, X):
            x_far(l, dx, src).start()
        x_mate(l, src).start()

    def gather_end(l, src):
        for dx in range(1, X):
            b = xbuf.at[((x - dx + X) % X) * 2 + c]
            rcopy(b, b, sX.at[l, dx], rX.at[l, dx], mate).wait_recv()
            x_relay(l, dx).start()
        b = xbuf.at[x * 2 + 1 - c]
        rcopy(b, b, sX.at[l, 0], rX.at[l, 0], mate).wait_recv()
        for dx in range(1, X):
            b = xbuf.at[((x - dx + X) % X) * 2 + 1 - c]
            rcopy(b, b, sXr.at[l, dx], rXr.at[l, dx], mate).wait_recv()
        x_mate(l, src).wait_send()
        for dx in range(1, X):
            x_far(l, dx, src).wait_send()
            x_relay(l, dx).wait_send()

    rows = 128 if Tk % 128 == 0 else Tk

    def norm(l):
        @pl.loop(0, Tk // rows)
        def _(r):
            at = pl.ds(pl.multiple_of(r * rows, rows), rows)
            total = jnp.zeros((rows, 1), F32)
            for k in range(TP):
                v = xbuf[k, at, :].astype(F32)
                total += jnp.sum(v * v, axis=1, keepdims=True)
            scale = lax.rsqrt(total / D + eps)
            for k in range(TP):
                cols = slice(k * Dt, (k + 1) * Dt)
                v = xbuf[k, at, :].astype(F32)
                nbuf[at, cols] = (v * scale * pre[l : l + 1, cols]).astype(BF16)

    tile = 256 if Ct % 256 == 0 else Ct

    def up(l):
        @pl.loop(0, Ct // tile)
        def _(j):
            cols = pl.ds(pl.multiple_of(j * tile, tile), tile)
            inner = jnp.dot(nbuf[...], wbuf[l, 0, :, cols], preferred_element_type=F32)
            value = jnp.dot(nbuf[...], wbuf[l, 1, :, cols], preferred_element_type=F32)
            gbuf[:, cols] = (inner * value).astype(BF16)
            oubuf[:, cols] = jnp.dot(nbuf[...], wbuf[l, 2, :, cols], preferred_element_type=F32)

    def halo(l, dev):
        return rcopy(gbuf.at[pl.ds(Tk - HALO, HALO)], hbuf.at[l], sH.at[l], rH.at[l], dev)

    def conv(l):
        @pl.when(s < SP - 1)
        def _():
            halo(l, (s + 1, t)).start()

        @pl.when(s > 0)
        def _():
            halo(l, (s - 1, t)).wait_recv()

        @pl.when(s == 0)
        def _():
            hbuf[l] = jnp.zeros((HALO, Ct), BF16)

        @pl.loop(0, Ct // 128)
        def _(j):
            cols = pl.ds(pl.multiple_of(j * 128, 128), 128)
            g = gbuf[:, cols].astype(F32)
            before = hbuf[l, :, cols].astype(F32)
            last, prev = before[HALO - 1 : HALO, :], before[HALO - 2 : HALO - 1, :]
            at = lax.broadcasted_iota(jnp.int32, g.shape, 0)
            g1 = jnp.where(at == 0, last, pltpu.roll(g, 1, 0))
            g2 = jnp.where(at == 0, prev, jnp.where(at == 1, last, pltpu.roll(g, 2, 0)))
            conv = g2 * taps[l, 0:1, cols] + g1 * taps[l, 1:2, cols] + g * taps[l, 2:3, cols]
            cbuf[:, cols] = (oubuf[:, cols] * conv).astype(BF16)

        @pl.when(s < SP - 1)
        def _():
            halo(l, (s + 1, t)).wait_send()

    nb = Dt // Ds

    def out_block(l, k):
        for b in range(nb):
            at = pl.ds(pl.multiple_of((k * nb + b) * Ct, Ct), Ct)
            pbuf[k, :, b * Ds : (b + 1) * Ds] = jnp.dot(
                cbuf[...], obuf[l, at, :], preferred_element_type=F32
            ).astype(BF16)

    def send_a(l, xx):
        return rcopy(pbuf.at[xx * 2 + 1 - c], pa.at[xx], sA.at[l, xx], rA.at[l, xx], mate)

    def send_b(l, dx):
        xx = (x + dx) % X
        return rcopy(pbuf.at[xx * 2 + c], pb.at[dx - 1], sB.at[l, dx], rB.at[l, dx], (s, xx * 2 + c))

    def send_p(l, d):
        return rcopy(pw.at[0], pw.at[d], sP.at[l, d], rP.at[l, d], (s, (t + d) % TP))

    def down(l):
        for dx in range(1, X + 1):
            xx = (x + dx) % X
            out_block(l, xx * 2 + 1 - c)
            send_a(l, xx).start()
        for dx in range(1, X):
            xx = (x + dx) % X
            k = xx * 2 + c
            out_block(l, k)
            send_a(l, xx).wait_recv()

            @pl.loop(0, Tk // rows)
            def _(r):
                at = pl.ds(pl.multiple_of(r * rows, rows), rows)
                pbuf[k, at, :] = (pbuf[k, at, :].astype(F32) + pa[xx, at, :].astype(F32)).astype(BF16)

            send_b(l, dx).start()
        out_block(l, t)

    def finish(l):
        send_a(l, x).wait_recv()
        for dx in range(1, X):
            send_b(l, dx).wait_recv()

        @pl.loop(0, Tk // rows)
        def _(r):
            at = pl.ds(pl.multiple_of(r * rows, rows), rows)
            total = pbuf[t, at, :].astype(F32) + pa[x, at, :].astype(F32)
            for dx in range(1, X):
                total += pb[dx - 1, at, :].astype(F32)
            mixed[at, :] = total
            power = jnp.sum(total * total, axis=1, keepdims=True)
            pw[0, :, at] = jnp.transpose(jnp.broadcast_to(power, (rows, 128)))[0:8, :]

        for d in range(1, TP):
            send_p(l, d).start()
        for d in range(1, TP):
            send_p(l, d).wait_recv()
        for d in range(1, TP):
            send_p(l, d).wait_send()
        for xx in range(X):
            send_a(l, xx).wait_send()
        for dx in range(1, X):
            send_b(l, dx).wait_send()

        @pl.loop(0, Tk // rows)
        def _(r):
            at = pl.ds(pl.multiple_of(r * rows, rows), rows)
            power = pw[0, :, at]
            for d in range(1, TP):
                power += pw[d, :, at]
            power = jnp.transpose(jnp.broadcast_to(power[0:1, :], (128, rows)))[:, 0:1]
            scale = lax.rsqrt(power / D + eps)
            new = xbuf[t, at, :].astype(F32) + mixed[at, :] * scale * post[l : l + 1, :]
            if l == L - 1:
                out_ref[at, :] = new.astype(BF16)
            else:
                xbuf[t, at, :] = new.astype(BF16)

    first = pltpu.make_async_copy(h_ref, xbuf.at[t], xsem)
    first.start()
    tau = 0
    advance(tau)
    gather_start(0, h_ref)
    last_tau = items - 1 + Z - 1

    def advance_to(upto):
        nonlocal tau
        while tau < min(upto, last_tau):
            tau += 1
            advance(tau)

    advance_to(2)
    first.wait()
    gather_end(0, h_ref)
    norm(0)
    for l in range(L):
        base = 4 * l
        advance_to(base + 2 + Z - 1)
        for m in range(3):
            arrived(base + m)
        up(l)
        conv(l)
        advance_to(base + 3 + Z - 1)
        arrived(base + 3)
        down(l)
        advance_to(base + 4 + Z - 1)
        finish(l)
        if l < L - 1:
            gather_start(l + 1, xbuf.at[t])
            advance_to(base + 5 + Z - 1)
            gather_end(l + 1, xbuf.at[t])
            norm(l + 1)

    for i in range(items):
        for h in range(Z - 1):
            @pl.when((z < Z - 1) & (z - h >= 0))
            def _():
                to_right(i, h).wait_send()

            @pl.when((z > 0) & (z + h <= Z - 1))
            def _():
                to_left(i, h).wait_send()

        for zb in range(Z):
            for d in range(1, Y):
                across(i, zb, d).wait_send()


def solution(mesh):
    SP, TP = mesh.shape["sp"], mesh.shape["tp"]

    def local(hidden_states, pre_gain, post_gain, w_value, w_outer, w_inner, taps, w_out):
        Tk, Dt = hidden_states.shape
        L, Ds, Ct = w_value.shape
        X = Y = TP // 2
        Z = SP // Y
        items = 4 * L
        dma = pltpu.SemaphoreType.DMA
        vmem = pl.BlockSpec(memory_space=pltpu.VMEM)
        hbm = pl.BlockSpec(memory_space=pltpu.HBM)
        return pl.pallas_call(
            functools.partial(kernel, SP, TP),
            out_shape=jax.ShapeDtypeStruct((Tk, Dt), BF16),
            in_specs=[hbm, vmem, vmem, hbm, hbm, hbm, vmem, hbm],
            out_specs=vmem,
            scratch_shapes=[
                pltpu.VMEM((L, 3, SP * Ds, Ct), BF16),
                pltpu.VMEM((L, SP * Ct, Ds), BF16),
                pltpu.VMEM((TP, Tk, Dt), BF16),
                pltpu.VMEM((Tk, Dt * TP), BF16),
                pltpu.VMEM((TP, Tk, Dt), BF16),
                pltpu.VMEM((X, Tk, Dt), BF16),
                pltpu.VMEM((max(X - 1, 1), Tk, Dt), BF16),
                pltpu.VMEM((Tk, Dt), F32),
                pltpu.VMEM((Tk, Ct), BF16),
                pltpu.VMEM((Tk, Ct), F32),
                pltpu.VMEM((L, HALO, Ct), BF16),
                pltpu.VMEM((Tk, Ct), BF16),
                pltpu.VMEM((TP, 8, Tk), F32),
                dma((items,)),
                dma((items, Z)), dma((items, Z)),
                dma((items, Z)), dma((items, Z)),
                dma((items, Z, Y)), dma((items, Z, Y)),
                dma((L, X)), dma((L, X)),
                dma((L, X)), dma((L, X)),
                dma((L, X)), dma((L, X)),
                dma((L, X)), dma((L, X)),
                dma((L, TP)), dma((L, TP)),
                dma((L,)), dma((L,)),
                dma,
            ],
            compiler_params=pltpu.CompilerParams(
                collective_id=0, has_side_effects=True, vmem_limit_bytes=67043328
            ),
        )(hidden_states, pre_gain, post_gain, w_value, w_outer, w_inner, taps, w_out)

    placed = (
        P("sp", "tp"),
        P(),
        P(None, "tp"),
        P(None, "sp", "tp"),
        P(None, "sp", "tp"),
        P(None, "sp", "tp"),
        P(None, None, "tp"),
        P(None, "tp", "sp"),
    )
    return jax.shard_map(
        local, mesh=mesh, in_specs=placed, out_specs=P("sp", "tp"), check_vma=False
    )
```

time: 730 us -> 409 us (0.56)
  waiting for transfers between devices: 641 us -> 0 us
  Pallas kernels: 0 us -> 405 us
  matrix products: 40.7 us -> 0 us
  other arithmetic: 14.9 us -> 0 us
  between operations: 13.7 us -> 0.01 us
  blocking collectives: 11.5 us -> 0 us
    all_gather x6 -> x0, waiting for transfers between devices: 548 us -> none  [the longest x1 124 us: local(): lax.all_gather(w_value, 'sp', axis=1, tiled=True)]
    pallas_call x0 -> x1, Pallas kernels: none -> 405 us  [local(): pl.pallas_call(functools.partial(kernel, SP, TP), out_shape=jax.ShapeDtyp...]
    reduce_scatter x2 -> x0, waiting for transfers between devices: 87.4 us -> none  [local(): lax.psum_scatter(partial_terms.astype(jnp.bfloat16), 'tp', scatter_dimens...]
    dot_general x8 -> x0, matrix products: 40.7 us -> none  [the longest x2 11 us: local(): jnp.dot(conv_out, whole_out[layer_index], preferred_element_type=jnp.floa...]
    psum x2 -> x0, blocking collectives: 11.5 us -> none  [local(): power = lax.psum(jnp.sum(mixed * mixed, axis=1), 'tp')]
    reduce_sum x4 -> x0, other arithmetic: 9.32 us -> none  [the longest x2 6.31 us: local(): jnp.mean(widened * widened, axis=1, keepdims=True) + eps]
  transfers between devices with their start and end apart: 10 -> 0, of which waited for: 10 -> 0; matrix products, arithmetic and copies ran while one was open for 3% -> 0% of each run, Pallas kernels for 0% -> 0%
where the time goes in v1:
time: 409 us
  Pallas kernels  405 us (99%)
    pallas_call x1, Pallas kernels, local(): pl.pallas_call(functools.partial(kernel, SP, TP), out_shape=jax.ShapeDtyp...  405 us

profile of v1, /device:TPU:0, one launch (start us, length us, event | category | flops | bytes accessed | tf_op | source)
XLA Modules:
  0.0 409.1 jit_solution(15644345894455039434)
XLA Ops:
  0.0 1.3 copy.9.taps
  1.3 405.5 %shard_map.82 = bf16[512,1024]{1,0:T(8,128)(2,1)} custom-call(bf16[512,1024]{1,0:T(8,128)(2,1)} %h_ref.1, f32[2,4096]{1,0:T(2,128)} %pre.1, f32[2,1024]{1,0:T(2,128)} %post.1, bf16[2,512,512]{2,1,0:T(8,128)(2,1)} %wv.1, bf16[2,512,512]{2,1,0:T(8,128)(2,1)} %wo.1, bf16[2,512,512]{2,1,0:T(8,128)(2,1)} %wi.1, f32[2,3,512]{2,1,0:T(4,128)} %copy.9.taps, ...), custom_call_target="tpu_custom_call" | custom-call | tf_op jit(solution)/shard_map/pallas_call | solution.py:370
  406.8 2.3 copy.11

commit v2 on v1

v2 whole, which is shorter than its diff:
```python
import functools

import jax
import jax.numpy as jnp
from jax import lax
from jax.experimental import pallas as pl
from jax.experimental.pallas import tpu as pltpu
from jax.sharding import PartitionSpec as P

MESH = pl.DeviceIdType.MESH
HALO = 16
eps = 1e-06
F32 = jnp.float32
BF16 = jnp.bfloat16


def layout(SP, TP, Ct):
    Y = 2 if SP % 2 == 0 and Ct % 256 == 0 else 1
    return Y, SP // Y, TP // 2


def kernel(
    SP, TP, h_ref, pre, post, wv, wo, wi, taps, wout, out_ref,
    wbuf, obuf, xbuf, nbuf, pbuf, pa, pb, mixed, gbuf, oubuf, hbuf, cbuf, pw,
    own_sem, sR, rR, sL, rL, sY, rY, sX, rX, sXr, rXr, sA, rA, sB, rB, sP, rP, sH, rH, xsem,
):
    Y, Z, X = layout(SP, TP, wv.shape[2])
    G = Y * X
    s = lax.axis_index("sp")
    t = lax.axis_index("tp")
    z, y = s // Y, s % Y
    x, c = t // 2, t % 2
    L, Ds, Ct = wv.shape
    Cv = Ct // Y
    Tk, Dt = h_ref.shape
    g = y * X + x
    D = Dt * TP
    items = 4 * L
    wrefs = (wi, wv, wo, wout)

    def rcopy(src, dst, ss, rs, dev):
        return pltpu.make_async_remote_copy(
            src_ref=src, dst_ref=dst, send_sem=ss, recv_sem=rs, device_id=dev, device_id_type=MESH
        )

    barrier = pltpu.get_barrier_semaphore()

    def hello(dev):
        pl.semaphore_signal(barrier, inc=1, device_id=dev, device_id_type=MESH)

    for by in (Y, SP - Y):
        hello(((s + by) % SP, t))
    for dy in range(Y):
        for d in range(TP):
            if dy or d:
                hello((z * Y + (y + dy) % Y, (t + d) % TP))
    pl.semaphore_wait(barrier, 2 + Y * TP - 1)

    def slot(i, b, n):
        l, m = divmod(i, 4)
        if m < 3:
            return wbuf.at[l, m, pl.ds(pl.multiple_of(b * Ds, Ds), n * Ds)]
        return obuf.at[l, pl.ds(pl.multiple_of(b * Cv, Cv), n * Cv)]

    def part(i, yy):
        l, m = divmod(i, 4)
        at = pl.ds(pl.multiple_of(yy * Cv, Cv), Cv)
        return wrefs[m].at[l, :, at] if m < 3 else wrefs[m].at[l, at]

    def to_right(i, h):
        b = slot(i, (z - h) * Y, Y)
        return rcopy(b, b, sR.at[i, h], rR.at[i, h], (s + Y, t))

    def to_left(i, h):
        b = slot(i, (z + h) * Y, Y)
        return rcopy(b, b, sL.at[i, h], rL.at[i, h], (s - Y, t))

    def from_left(i, h):
        b = slot(i, (z - 1 - h) * Y, Y)
        return rcopy(b, b, sR.at[i, h], rR.at[i, h], (s - Y, t))

    def from_right(i, h):
        b = slot(i, (z + 1 + h) * Y, Y)
        return rcopy(b, b, sL.at[i, h], rL.at[i, h], (s + Y, t))

    def across(i, d):
        yy = (y + d) % Y
        return rcopy(part(i, yy), slot(i, s, 1), sY.at[i, d], rY.at[i, d], (z * Y + yy, t))

    def from_across(i, d):
        b = slot(i, z * Y + (y - d + Y) % Y, 1)
        return rcopy(b, b, sY.at[i, d], rY.at[i, d], (z * Y + (y + d) % Y, t))

    def own_copy(i):
        return pltpu.make_async_copy(part(i, y), slot(i, s, 1), own_sem.at[i])

    def exchange(i):
        own_copy(i).start()
        for d in range(1, Y):
            across(i, d).start()

    def stage(i, h):
        if h == 0:
            own_copy(i).wait()
            for d in range(1, Y):
                from_across(i, d).wait_recv()

            @pl.when(z < Z - 1)
            def _():
                to_right(i, 0).start()

            @pl.when(z > 0)
            def _():
                to_left(i, 0).start()

            return

        @pl.when(z - h >= 0)
        def _():
            from_left(i, h - 1).wait_recv()
            if h <= Z - 2:
                @pl.when(z < Z - 1)
                def _():
                    to_right(i, h).start()

        @pl.when(z + h <= Z - 1)
        def _():
            from_right(i, h - 1).wait_recv()
            if h <= Z - 2:
                @pl.when(z > 0)
                def _():
                    to_left(i, h).start()

    begins = [min(i, items - 2) for i in range(items)]

    def advance(tau):
        for i in range(items):
            if 0 <= tau - begins[i] <= Z - 1:
                stage(i, tau - begins[i])

    mate = (s, x * 2 + 1 - c)

    def dev(gg, cc):
        return (z * Y + gg // X, (gg % X) * 2 + cc)

    me = g * 2 + c

    def x_mate(l, src):
        return rcopy(src, xbuf.at[me], sX.at[l, 0], rX.at[l, 0], mate)

    def x_far(l, d, src):
        return rcopy(src, xbuf.at[me], sX.at[l, d], rX.at[l, d], dev((g + d) % G, c))

    def x_relay(l, d):
        b = xbuf.at[((g - d + G) % G) * 2 + c]
        return rcopy(b, b, sXr.at[l, d], rXr.at[l, d], mate)

    def gather_start(l, src):
        for d in range(1, G):
            x_far(l, d, src).start()
        x_mate(l, src).start()

    def gather_end(l, src, between):
        for d in range(1, G):
            b = xbuf.at[((g - d + G) % G) * 2 + c]
            rcopy(b, b, sX.at[l, d], rX.at[l, d], mate).wait_recv()
            x_relay(l, d).start()
            if d == 1:
                between()
        b = xbuf.at[g * 2 + 1 - c]
        rcopy(b, b, sX.at[l, 0], rX.at[l, 0], mate).wait_recv()
        for d in range(1, G):
            b = xbuf.at[((g - d + G) % G) * 2 + 1 - c]
            rcopy(b, b, sXr.at[l, d], rXr.at[l, d], mate).wait_recv()
        x_mate(l, src).wait_send()
        for d in range(1, G):
            x_far(l, d, src).wait_send()
            x_relay(l, d).wait_send()

    rows = 128 if Tk % 128 == 0 else Tk

    def norm(l):
        for yy in range(Y):
            @pl.loop(0, Tk // rows)
            def _(r):
                at = pl.ds(pl.multiple_of(r * rows, rows), rows)
                to = pl.ds(pl.multiple_of(yy * Tk + r * rows, rows), rows)
                total = jnp.zeros((rows, 1), F32)
                for k in range(TP):
                    v = xbuf[yy * TP + k, at, :].astype(F32)
                    total += jnp.sum(v * v, axis=1, keepdims=True)
                scale = lax.rsqrt(total / D + eps)
                for k in range(TP):
                    cols = slice(k * Dt, (k + 1) * Dt)
                    v = xbuf[yy * TP + k, at, :].astype(F32)
                    nbuf[to, cols] = (v * scale * pre[l : l + 1, cols]).astype(BF16)

    def up(l):
        @pl.loop(0, Y)
        def _(j):
            at = pl.ds(pl.multiple_of(j * Tk, Tk), Tk)
            inner = jnp.dot(nbuf[at, :], wbuf[l, 0], preferred_element_type=F32)
            value = jnp.dot(nbuf[at, :], wbuf[l, 1], preferred_element_type=F32)
            gbuf[at, :] = (inner * value).astype(BF16)
            oubuf[at, :] = jnp.dot(nbuf[at, :], wbuf[l, 2], preferred_element_type=F32)

    def halo(l, dev):
        return rcopy(gbuf.at[pl.ds(Y * Tk - HALO, HALO)], hbuf.at[l], sH.at[l], rH.at[l], dev)

    def conv(l):
        @pl.when(z < Z - 1)
        def _():
            halo(l, (s + Y, t)).start()

        @pl.when(z > 0)
        def _():
            halo(l, (s - Y, t)).wait_recv()

        @pl.when(z == 0)
        def _():
            hbuf[l] = jnp.zeros((HALO, Cv), BF16)

        @pl.loop(0, Cv // 128)
        def _(j):
            cols = pl.ds(pl.multiple_of(j * 128, 128), 128)
            mine = pl.ds(pl.multiple_of(y * Cv + j * 128, 128), 128)
            v = gbuf[:, cols].astype(F32)
            before = hbuf[l, :, cols].astype(F32)
            last, prev = before[HALO - 1 : HALO, :], before[HALO - 2 : HALO - 1, :]
            at = lax.broadcasted_iota(jnp.int32, v.shape, 0)
            g1 = jnp.where(at == 0, last, pltpu.roll(v, 1, 0))
            g2 = jnp.where(at == 0, prev, jnp.where(at == 1, last, pltpu.roll(v, 2, 0)))
            conv = g2 * taps[l, 0:1, mine] + g1 * taps[l, 1:2, mine] + v * taps[l, 2:3, mine]
            cbuf[:, cols] = (oubuf[:, cols] * conv).astype(BF16)

        @pl.when(z < Z - 1)
        def _():
            halo(l, (s + Y, t)).wait_send()

    nb = Dt // Ds

    def out_block(l, gg, cc):
        yy, tt = gg // X, (gg % X) * 2 + cc
        at = pl.ds(pl.multiple_of(yy * Tk, Tk), Tk)
        for b in range(nb):
            of = pl.ds(pl.multiple_of((tt * nb + b) * Cv, Cv), Cv)
            pbuf[gg * 2 + cc, :, b * Ds : (b + 1) * Ds] = jnp.dot(
                cbuf[at, :], obuf[l, of, :], preferred_element_type=F32
            ).astype(BF16)

    def send_a(l, xx):
        return rcopy(pbuf.at[xx * 2 + 1 - c], pa.at[xx], sA.at[l, xx], rA.at[l, xx], mate)

    def send_b(l, dx):
        gg = (g + dx) % G
        return rcopy(pbuf.at[gg * 2 + c], pb.at[dx - 1], sB.at[l, dx], rB.at[l, dx], dev(gg, c))

    def send_p(l, d):
        return rcopy(pw.at[0], pw.at[d], sP.at[l, d], rP.at[l, d], (s, (t + d) % TP))

    def down(l):
        for dx in range(1, G + 1):
            xx = (g + dx) % G
            out_block(l, xx, 1 - c)
            send_a(l, xx).start()
        for dx in range(1, G):
            xx = (g + dx) % G
            k = xx * 2 + c
            out_block(l, xx, c)
            send_a(l, xx).wait_recv()

            @pl.loop(0, Tk // rows)
            def _(r):
                at = pl.ds(pl.multiple_of(r * rows, rows), rows)
                pbuf[k, at, :] = (pbuf[k, at, :].astype(F32) + pa[xx, at, :].astype(F32)).astype(BF16)

            send_b(l, dx).start()
        out_block(l, g, c)

    def finish(l, between):
        send_a(l, g).wait_recv()
        for dx in range(1, G):
            send_b(l, dx).wait_recv()
            if dx == 1:
                between()

        @pl.loop(0, Tk // rows)
        def _(r):
            at = pl.ds(pl.multiple_of(r * rows, rows), rows)
            total = pbuf[me, at, :].astype(F32) + pa[g, at, :].astype(F32)
            for dx in range(1, G):
                total += pb[dx - 1, at, :].astype(F32)
            mixed[at, :] = total
            power = jnp.sum(total * total, axis=1, keepdims=True)
            pw[0, :, at] = jnp.transpose(jnp.broadcast_to(power, (rows, 128)))[0:8, :]

        for d in range(1, TP):
            send_p(l, d).start()
        for d in range(1, TP):
            send_p(l, d).wait_recv()
        for d in range(1, TP):
            send_p(l, d).wait_send()
        for xx in range(G):
            send_a(l, xx).wait_send()
        for dx in range(1, G):
            send_b(l, dx).wait_send()

        @pl.loop(0, Tk // rows)
        def _(r):
            at = pl.ds(pl.multiple_of(r * rows, rows), rows)
            power = pw[0, :, at]
            for d in range(1, TP):
                power += pw[d, :, at]
            power = jnp.transpose(jnp.broadcast_to(power[0:1, :], (128, rows)))[:, 0:1]
            scale = lax.rsqrt(power / D + eps)
            new = xbuf[me, at, :].astype(F32) + mixed[at, :] * scale * post[l : l + 1, :]
            if l == L - 1:
                out_ref[at, :] = new.astype(BF16)
            else:
                xbuf[me, at, :] = new.astype(BF16)

    first = pltpu.make_async_copy(h_ref, xbuf.at[me], xsem)
    first.start()
    exchanged = 0
    tau = -1
    last_tau = begins[-1] + Z - 1

    def advance_to(upto):
        nonlocal tau, exchanged
        while tau < min(upto, last_tau):
            tau += 1
            while exchanged < items and begins[exchanged] <= tau + 2:
                exchange(exchanged)
                exchanged += 1
            advance(tau)

    advance_to(0)
    gather_start(0, h_ref)
    advance_to(1)
    first.wait()
    gather_end(0, h_ref, lambda: advance_to(2))
    advance_to(3)
    norm(0)
    for l in range(L):
        base = 4 * l
        advance_to(begins[base + 2] + Z - 1)
        up(l)
        conv(l)
        advance_to(begins[base + 3] + Z - 1)
        down(l)
        finish(l, lambda: advance_to(base + 4 + Z - 1))
        if l < L - 1:
            gather_start(l + 1, xbuf.at[me])
            advance_to(base + 5 + Z - 1)
            gather_end(l + 1, xbuf.at[me], lambda: advance_to(base + 6 + Z - 1))
            norm(l + 1)

    for i in range(items):
        for h in range(Z - 1):
            @pl.when((z < Z - 1) & (z - h >= 0))
            def _():
                to_right(i, h).wait_send()

            @pl.when((z > 0) & (z + h <= Z - 1))
            def _():
                to_left(i, h).wait_send()

        for d in range(1, Y):
            across(i, d).wait_send()


def solution(mesh):
    SP, TP = mesh.shape["sp"], mesh.shape["tp"]

    def local(hidden_states, pre_gain, post_gain, w_value, w_outer, w_inner, taps, w_out):
        Tk, Dt = hidden_states.shape
        L, Ds, Ct = w_value.shape
        Y, Z, X = layout(SP, TP, Ct)
        G, Cv = X * Y, Ct // Y
        items = 4 * L
        dma = pltpu.SemaphoreType.DMA
        vmem = pl.BlockSpec(memory_space=pltpu.VMEM)
        hbm = pl.BlockSpec(memory_space=pltpu.HBM)
        return pl.pallas_call(
            functools.partial(kernel, SP, TP),
            out_shape=jax.ShapeDtypeStruct((Tk, Dt), BF16),
            in_specs=[hbm, vmem, vmem, hbm, hbm, hbm, vmem, hbm],
            out_specs=vmem,
            scratch_shapes=[
                pltpu.VMEM((L, 3, SP * Ds, Cv), BF16),
                pltpu.VMEM((L, SP * Cv, Ds), BF16),
                pltpu.VMEM((G * 2, Tk, Dt), BF16),
                pltpu.VMEM((Y * Tk, Dt * TP), BF16),
                pltpu.VMEM((G * 2, Tk, Dt), BF16),
                pltpu.VMEM((G, Tk, Dt), BF16),
                pltpu.VMEM((max(G - 1, 1), Tk, Dt), BF16),
                pltpu.VMEM((Tk, Dt), F32),
                pltpu.VMEM((Y * Tk, Cv), BF16),
                pltpu.VMEM((Y * Tk, Cv), F32),
                pltpu.VMEM((L, HALO, Cv), BF16),
                pltpu.VMEM((Y * Tk, Cv), BF16),
                pltpu.VMEM((TP, 8, Tk), F32),
                dma((items,)),
                dma((items, Z)), dma((items, Z)),
                dma((items, Z)), dma((items, Z)),
                dma((items, Y)), dma((items, Y)),
                dma((L, G)), dma((L, G)),
                dma((L, G)), dma((L, G)),
                dma((L, G)), dma((L, G)),
                dma((L, G)), dma((L, G)),
                dma((L, TP)), dma((L, TP)),
                dma((L,)), dma((L,)),
                dma,
            ],
            compiler_params=pltpu.CompilerParams(
                collective_id=0, has_side_effects=True, vmem_limit_bytes=67043328
            ),
        )(hidden_states, pre_gain, post_gain, w_value, w_outer, w_inner, taps, w_out)

    placed = (
        P("sp", "tp"),
        P(),
        P(None, "tp"),
        P(None, "sp", "tp"),
        P(None, "sp", "tp"),
        P(None, "sp", "tp"),
        P(None, None, "tp"),
        P(None, "tp", "sp"),
    )
    return jax.shard_map(
        local, mesh=mesh, in_specs=placed, out_specs=P("sp", "tp"), check_vma=False
    )
```

time: 409 us -> 371 us (0.907)
  Pallas kernels: 405 us -> 367 us
    pallas_call x1, Pallas kernels: 405 us -> 367 us  [local(): pl.pallas_call(functools.partial(kernel, SP, TP), out_shape=jax.ShapeDtyp...]
where the time goes in v2:
time: 371 us
  Pallas kernels  367 us (99%)
    pallas_call x1, Pallas kernels, local(): pl.pallas_call(functools.partial(kernel, SP, TP), out_shape=jax.ShapeDtyp...  367 us

profile of v2, /device:TPU:0, one launch (start us, length us, event | category | flops | bytes accessed | tf_op | source)
XLA Modules:
  0.0 370.5 jit_solution(1989381010579489138)
XLA Ops:
  0.0 1.3 copy.9.taps
  1.3 366.9 %shard_map.82 = bf16[512,1024]{1,0:T(8,128)(2,1)} custom-call(bf16[512,1024]{1,0:T(8,128)(2,1)} %h_ref.1, f32[2,4096]{1,0:T(2,128)} %pre.1, f32[2,1024]{1,0:T(2,128)} %post.1, bf16[2,512,512]{2,1,0:T(8,128)(2,1)} %wv.1, bf16[2,512,512]{2,1,0:T(8,128)(2,1)} %wo.1, bf16[2,512,512]{2,1,0:T(8,128)(2,1)} %wi.1, f32[2,3,512]{2,1,0:T(4,128)} %copy.9.taps, ...), custom_call_target="tpu_custom_call" | custom-call | tf_op jit(solution)/shard_map/pallas_call | solution.py:384
  368.2 2.3 copy.11

commit v3 on v2

--- a/solution.py
+++ b/solution.py
@@ -131,11 +131,11 @@
                 def _():
                     to_left(i, h).start()
 
-    begins = [min(i, items - 2) for i in range(items)]
-
-    def advance(tau):
+    begins = list(range(items))
+
+    def advance(tau, skip=-1):
         for i in range(items):
-            if 0 <= tau - begins[i] <= Z - 1:
+            if i != skip and 0 <= tau - begins[i] <= Z - 1:
                 stage(i, tau - begins[i])
 
     mate = (s, x * 2 + 1 - c)
@@ -195,23 +195,29 @@
                     v = xbuf[yy * TP + k, at, :].astype(F32)
                     nbuf[to, cols] = (v * scale * pre[l : l + 1, cols]).astype(BF16)
 
-    def up(l):
+    def up_gate(l):
         @pl.loop(0, Y)
         def _(j):
             at = pl.ds(pl.multiple_of(j * Tk, Tk), Tk)
             inner = jnp.dot(nbuf[at, :], wbuf[l, 0], preferred_element_type=F32)
             value = jnp.dot(nbuf[at, :], wbuf[l, 1], preferred_element_type=F32)
             gbuf[at, :] = (inner * value).astype(BF16)
+
+    def up_outer(l):
+        @pl.loop(0, Y)
+        def _(j):
+            at = pl.ds(pl.multiple_of(j * Tk, Tk), Tk)
             oubuf[at, :] = jnp.dot(nbuf[at, :], wbuf[l, 2], preferred_element_type=F32)
 
     def halo(l, dev):
         return rcopy(gbuf.at[pl.ds(Y * Tk - HALO, HALO)], hbuf.at[l], sH.at[l], rH.at[l], dev)
 
+    def halo_start(l):
+        @pl.when(z < Z - 1)
+        def _():
+            halo(l, (s + Y, t)).start()
+
     def conv(l):
-        @pl.when(z < Z - 1)
-        def _():
-            halo(l, (s + Y, t)).start()
-
         @pl.when(z > 0)
         def _():
             halo(l, (s - Y, t)).wait_recv()
@@ -277,8 +283,48 @@
             send_b(l, dx).start()
         out_block(l, g, c)
 
+    by_block = SP == Y * TP
+
+    def down_block(l, tt):
+        cc = tt % 2
+        for yy in range(Y):
+            gg = yy * X + tt // 2
+            out_block(l, gg, cc)
+
+            @pl.when(cc != c)
+            def _():
+                send_a(l, gg).start()
+
+            @pl.when(cc == c)
+            def _():
+                send_a(l, gg).wait_recv()
+
+                @pl.when(gg != g)
+                def _():
+                    @pl.loop(0, Tk // rows)
+                    def _(r):
+                        at = pl.ds(pl.multiple_of(r * rows, rows), rows)
+                        k = gg * 2 + c
+                        pbuf[k, at, :] = (pbuf[k, at, :].astype(F32) + pa[gg, at, :].astype(F32)).astype(BF16)
+
+                    send_b(l, (gg - g + G) % G).start()
+
+    def down_step(l, h):
+        if h == 0:
+            down_block(l, z)
+            return
+
+        @pl.when(z - h >= 0)
+        def _():
+            down_block(l, z - h)
+
+        @pl.when(z + h <= Z - 1)
+        def _():
+            down_block(l, z + h)
+
     def finish(l, between):
-        send_a(l, g).wait_recv()
+        if not by_block:
+            send_a(l, g).wait_recv()
         for dx in range(1, G):
             send_b(l, dx).wait_recv()
             if dx == 1:
@@ -325,14 +371,14 @@
     tau = -1
     last_tau = begins[-1] + Z - 1
 
-    def advance_to(upto):
+    def advance_to(upto, skip=-1):
         nonlocal tau, exchanged
         while tau < min(upto, last_tau):
             tau += 1
             while exchanged < items and begins[exchanged] <= tau + 2:
                 exchange(exchanged)
                 exchanged += 1
-            advance(tau)
+            advance(tau, skip)
 
     advance_to(0)
     gather_start(0, h_ref)
@@ -343,16 +389,37 @@
     norm(0)
     for l in range(L):
         base = 4 * l
-        advance_to(begins[base + 2] + Z - 1)
-        up(l)
+        advance_to(begins[base + 1] + Z - 1)
+        up_gate(l)
+        halo_start(l)
+        late = base + 3 if l == L - 1 and by_block and Z > 2 else -1
+        advance_to(begins[base + 2] + Z - 1, late)
+        if late >= 0:
+            @pl.when((z > 0) & (z < Z - 1))
+            def _():
+                stage(late, Z - 2)
+
+        up_outer(l)
         conv(l)
-        advance_to(begins[base + 3] + Z - 1)
-        down(l)
+        if by_block:
+            for h in range(Z - 2):
+                down_step(l, h)
+            if late >= 0:
+                @pl.when((z == 0) | (z == Z - 1))
+                def _():
+                    stage(late, Z - 2)
+
+            if Z > 1:
+                down_step(l, Z - 2)
+            advance_to(begins[base + 3] + Z - 1)
+            down_step(l, Z - 1)
+        else:
+            advance_to(begins[base + 3] + Z - 1)
+            down(l)
         finish(l, lambda: advance_to(base + 4 + Z - 1))
         if l < L - 1:
             gather_start(l + 1, xbuf.at[me])
-            advance_to(base + 5 + Z - 1)
-            gather_end(l + 1, xbuf.at[me], lambda: advance_to(base + 6 + Z - 1))
+            gather_end(l + 1, xbuf.at[me], lambda: advance_to(base + 5 + Z - 1))
             norm(l + 1)
 
     for i in range(items):

time: 371 us -> 368 us (level); the launches traced: 371 us -> 361 us
  Pallas kernels: 367 us -> 358 us
    pallas_call x1, Pallas kernels: 367 us -> 358 us  [local(): pl.pallas_call(functools.partial(kernel, SP, TP), out_shape=jax.ShapeDtyp...]
where the time goes in v3:
time: 368 us; the launch traced here: 361 us
  Pallas kernels  358 us (97%)
    pallas_call x1, Pallas kernels, local(): pl.pallas_call(functools.partial(kernel, SP, TP), out_shape=jax.ShapeDtyp...  358 us

profile of v3, /device:TPU:0, one launch (start us, length us, event | category | flops | bytes accessed | tf_op | source)
XLA Modules:
  0.0 361.2 jit_solution(9487910852629229634)
XLA Ops:
  0.0 1.3 copy.9.taps
  1.3 357.6 %shard_map.82 = bf16[512,1024]{1,0:T(8,128)(2,1)} custom-call(bf16[512,1024]{1,0:T(8,128)(2,1)} %h_ref.1, f32[2,4096]{1,0:T(2,128)} %pre.1, f32[2,1024]{1,0:T(2,128)} %post.1, bf16[2,512,512]{2,1,0:T(8,128)(2,1)} %wv.1, bf16[2,512,512]{2,1,0:T(8,128)(2,1)} %wo.1, bf16[2,512,512]{2,1,0:T(8,128)(2,1)} %wi.1, f32[2,3,512]{2,1,0:T(4,128)} %copy.9.taps, ...), custom_call_target="tpu_custom_call" | custom-call | tf_op jit(solution)/shard_map/pallas_call | solution.py:451
  358.9 2.3 copy.11
